TPU v7x, 256 devices: a 4x2x16 block of a 4x16x16 slice. The times are simulated.
256 devices in a mesh: grp: 2 (over y), sp: 32 (over z, core), tp: 4 (over x).
Axes of the slice: x: 4, y: 2, z: 16, core: 2. Of those that a mesh axis runs over, the one named last changes fastest.
The devices are a block of a 4x16x16 slice.
Arguments:
- queries: bfloat16 [14336, 1024], P(('grp', 'sp'), 'tp'), parts along dimension 0, may hold values from -6 to 6
- head_key_rows: bfloat16 [14336, 1024], P(('grp', 'sp'), 'tp'), parts along dimension 0, may hold values from -6 to 6
- head_value_rows: bfloat16 [14336, 2048], P(('grp', 'sp'), 'tp'), parts along dimension 0, may hold values from -6 to 6
- input_gate_logit: float32 [16, 14336], P('tp', ('grp', 'sp')), parts along dimension 1, may hold values from -6 to 300
- forget_gate_preact: float32 [16, 14336], P('tp', ('grp', 'sp')), parts along dimension 1, may hold values from 0 to 14
- forget_log_offset: float32 [16, 14336], P('tp', ('grp', 'sp')), parts along dimension 1, may hold values from -0.7 to 0
- per_head_norm_gain: bfloat16 [2048], P('tp'), may hold values from 0.099609375 to 1.8984375
- cell_output_matrix: bfloat16 [2048, 2048], P('tp', 'sp'), may hold values from -0.125 to 0.125
- layer_input_rows: bfloat16 [14336, 2048], P(('grp', 'sp', 'tp')), parts along dimension 0, may hold values from -6 to 6
- expert_norm_gain: bfloat16 [2048], replicated, may hold values from 0.099609375 to 1.8984375
- chosen_expert_index: int32 [14336, 2], P(('grp', 'sp', 'tp')), parts along dimension 0, may hold values from 0 to 31, all different within a row; in each aligned block of 56 rows (0 to 55, 56 to 111, ...) at most 7 rows name the same one
- chosen_expert_weight: float32 [14336, 2], P(('grp', 'sp', 'tp')), parts along dimension 0, may hold values from 0.2 to 1
- expert_gate_matrix: bfloat16 [32, 2048, 3584], P('sp', None, 'tp'), may hold values from -0.125 to 0.125
- expert_up_matrix: bfloat16 [32, 2048, 3584], P('sp', None, 'tp'), may hold values from -0.125 to 0.125
- expert_down_matrix: bfloat16 [32, 3584, 2048], P('sp', 'tp'), may hold values from -0.09375 to 0.09375
Outputs:
- layer_out: bfloat16 [14336, 2048], P(('grp', 'sp', 'tp')), parts along dimension 0
There are 2 independent parts, one for each index of `grp`. A program takes and returns all parts, laid end to end along the dimension named above; an argument that names none is the same for every part. Nothing has to cross between parts.
Inputs may be any that keep to these rules, and one draw needn't show every extreme that they name: `chosen_expert_index`: each row names 2 different experts. In the rows of one device no expert is named more than 7 times, and in every draw some expert is named exactly 7 times in the rows of some device.
All inputs are finite; a program needn't handle non-finite values.
Results may differ from a plain program's by a relative error of at most 0.013.
Values may be sent and summed in bfloat16 or wider, within the bound.
No kernel may reach another device: no remote copies, remote signals or barrier semaphores. Data moves between devices by JAX's collectives and lax.ppermute only.
A program may use at most 64 MiB of HBM per device.

v0:
```python
import jax
import jax.numpy as jnp
from jax import lax
from jax.sharding import Mesh
from jax.sharding import PartitionSpec as P

DK = 64
DV = 128
SP = ("sp_0", "sp_1")
GRP_SP = ("grp", "sp_0", "sp_1")
GRP_SP_TP = ("grp", "sp_0", "sp_1", "tp")
far_below = -1e30
norm_eps = 1e-06


def all_in_one(x, axis):
    leaves = jax.tree.leaves(x)
    turns = sorted(range(len(leaves)), key=lambda k: -leaves[k].size)
    width = (1, *leaves[turns[0]].shape)[-1]
    lines = [
        jnp.pad(leaves[k].reshape(-1), (0, -leaves[k].size % width)).reshape(-1, width)
        for k in turns
    ]
    both, at, found = (lax.all_gather(jnp.concatenate(lines), axis), 0, {})
    for k, line in zip(turns, lines):
        slab = both[:, at : at + len(line)].reshape(len(both), -1)
        found[k] = slab[:, : leaves[k].size].reshape(-1, *leaves[k].shape)
        at += len(line)
    numbers = iter(range(len(leaves)))
    return jax.tree.map(lambda _: found[next(numbers)], x)


def carried_in(part, axis, combine, identity):
    place = lax.axis_index(axis)
    gathered = all_in_one(part, axis)
    state = jax.tree.map(lambda a, e: jnp.zeros_like(a) + jnp.asarray(e, a.dtype), part, identity)

    def one(lap, state):
        return combine(
            state, jax.tree.map(lambda a: lax.dynamic_index_in_dim(a, lap, 0, False), gathered)
        )

    return lax.fori_loop(0, place, one, state)


def cut_along(x, dim, size):
    before, after = (x.shape[:dim], x.shape[dim + 1 :])
    return jnp.moveaxis(x.reshape(*before, size, -1, *after), dim, 0)


def summed_on_arrival(x, axis, dim):
    size = lax.axis_size(axis)
    tiles = lax.all_to_all(cut_along(x, dim, size), axis, 0, 0, tiled=True)
    return jnp.sum(tiles.astype(jnp.float32), axis=0)


def from_everyone(x, axis):
    copies = jnp.broadcast_to(x, (lax.axis_size(axis), *x.shape))
    return lax.all_to_all(copies, axis, split_axis=0, concat_axis=0, tiled=True)


def joined_along(tiles, dim):
    dims = list(tiles.shape[1:])
    dims[dim] *= tiles.shape[0]
    return jnp.moveaxis(tiles, 0, dim).reshape(dims)


def collect(x, axis, dim):
    tiles = from_everyone(x, axis)
    return joined_along(tiles, dim)


def exchange_in_order(tiles, axes, turns):
    dims = [lax.axis_size(a) for a in axes]
    tiles = tiles.reshape(*dims, *tiles.shape[1:])
    for k in turns:
        tiles = lax.all_to_all(tiles, axes[k], split_axis=k, concat_axis=k, tiled=True)
    return tiles.reshape(-1, *tiles.shape[len(axes) :])


def exchange_by_chip(x, groups, turns, split_dim, concat_dim):
    size = lax.axis_size(groups[0]) * lax.axis_size(groups[1])
    tiles = cut_along(x, split_dim, size)
    return joined_along(exchange_in_order(tiles, groups, turns), concat_dim)


def items_in_groups(x, axis, split_dim, concat_dim, work, item_dim, out_dim):
    items = jax.tree.leaves(x)[0].shape[item_dim]
    count = 2 if items % 2 == 0 else 1
    finished = []
    for k in range(count):
        group = jax.tree.map(
            lambda a: lax.slice_in_dim(
                a, k * (items // count), (k + 1) * (items // count), axis=item_dim
            ),
            x,
        )
        finished.append(
            work(
                lax.all_to_all(
                    group, axis, split_axis=split_dim, concat_axis=concat_dim, tiled=True
                )
            )
        )
    return jax.tree.map(lambda *parts: jnp.concatenate(parts, axis=out_dim), *finished)


def combine_states(earlier, later):
    total_a, memory_a, peak_a = earlier
    total_b, memory_b, peak_b = later
    peak = jnp.maximum(total_b + peak_a, peak_b)
    weight_a = jnp.exp(total_b + peak_a - peak)
    weight_b = jnp.exp(peak_b - peak)
    memory = weight_a[:, None, None] * memory_a + weight_b[:, None, None] * memory_b
    return (total_a + total_b, memory, peak)


def block_summary(keys3, values3, log_in, log_retention):
    running = jnp.cumsum(log_retention, axis=1)
    totals = running[:, -1]
    term_log = totals[:, None] - running + log_in
    peak = jnp.max(term_log, axis=1)
    factors = jnp.transpose(jnp.exp(term_log - peak[:, None]))
    keys32 = keys3.astype(jnp.float32)
    weighted = values3.astype(jnp.float32) * factors[:, :, None]
    memory = jnp.einsum("shd,she->hde", keys32, weighted, precision=lax.Precision.HIGHEST)
    return (totals, memory, peak)


def block_output(queries3, keys3, values3, log_in, log_retention, state, gains):
    count = queries3.shape[0]
    heads = queries3.shape[1]
    memory_in, peak_in = (state[1], state[2])
    running = jnp.cumsum(log_retention, axis=1)
    rows_at = lax.broadcasted_iota(jnp.int32, (count, count), 0)
    cols_at = lax.broadcasted_iota(jnp.int32, (count, count), 1)
    causal = (cols_at <= rows_at)[None]
    decay_log = jnp.where(
        causal, running[:, :, None] - running[:, None, :] + log_in[:, None, :], far_below
    )
    carried_log = running + peak_in[:, None]
    peak = jnp.maximum(carried_log, jnp.max(decay_log, axis=2))
    qk_scale = queries3.shape[2] ** (-0.5)
    scores = (
        jnp.einsum("thd,shd->hts", queries3, keys3, preferred_element_type=jnp.float32) * qk_scale
    )
    strength = scores * jnp.exp(decay_log - peak[:, :, None])
    carried = jnp.exp(carried_log - peak)
    queries32 = queries3.astype(jnp.float32)
    from_memory = (
        jnp.einsum("thd,hde->the", queries32, memory_in, precision=lax.Precision.HIGHEST) * qk_scale
    )
    within = jnp.einsum(
        "hts,she->the", strength.astype(jnp.bfloat16), values3, preferred_element_type=jnp.float32
    )
    result = within + jnp.transpose(carried)[:, :, None] * from_memory
    result = result * lax.rsqrt(jnp.mean(result * result, axis=2, keepdims=True) + norm_eps)
    result = result * gains.astype(jnp.float32).reshape(heads, -1)
    return result.reshape(count, -1).astype(jnp.bfloat16)


def run_expert(rows_in, expert_gate_matrix, expert_up_matrix, expert_down_matrix):
    gate = jnp.dot(rows_in, expert_gate_matrix[0], preferred_element_type=jnp.float32)
    upward = jnp.dot(rows_in, expert_up_matrix[0], preferred_element_type=jnp.float32)
    hidden = (jax.nn.silu(gate) * upward).astype(jnp.bfloat16)
    return jnp.dot(hidden, expert_down_matrix[0], preferred_element_type=jnp.float32)


def shards(
    queries,
    head_key_rows,
    head_value_rows,
    input_gate_logit,
    forget_gate_preact,
    forget_log_offset,
    per_head_norm_gain,
    cell_output_matrix,
    layer_input_rows,
    expert_norm_gain,
    chosen_expert_index,
    chosen_expert_weight,
    expert_gate_matrix,
    expert_up_matrix,
    expert_down_matrix,
):
    count = queries.shape[0]
    heads = input_gate_logit.shape[0]
    queries3 = queries.reshape(count, heads, DK)
    keys3 = head_key_rows.reshape(count, heads, DK)
    values3 = head_value_rows.reshape(count, heads, DV)
    log_retention = jax.nn.log_sigmoid(forget_gate_preact) + forget_log_offset
    summary = block_summary(keys3, values3, input_gate_logit, log_retention)
    identity = (
        jnp.zeros((heads,), jnp.float32),
        jnp.zeros((heads, DK, DV), jnp.float32),
        jnp.full((heads,), far_below, jnp.float32),
    )
    incoming = carried_in(summary, SP, combine_states, identity)
    mixed = block_output(
        queries3, keys3, values3, input_gate_logit, log_retention, incoming, per_head_norm_gain
    )
    partial_value = jnp.dot(
        mixed,
        lax.all_gather(cell_output_matrix, SP, axis=1, tiled=True),
        preferred_element_type=jnp.float32,
    )
    projected = summed_on_arrival(partial_value.astype(jnp.bfloat16), "tp", 0)
    residual = layer_input_rows.astype(jnp.float32) + projected
    normed = residual * lax.rsqrt(jnp.mean(residual * residual, axis=1, keepdims=True) + norm_eps)
    normed = (normed * expert_norm_gain.astype(jnp.float32)).astype(jnp.bfloat16)
    rows = layer_input_rows.shape[0]
    model_width = layer_input_rows.shape[1]
    experts = lax.axis_size(SP)
    slots = max(2, (4 * rows + experts - 1) // experts)
    flat_ids = chosen_expert_index.reshape(rows * 2)
    onehot = (flat_ids[:, None] == jnp.arange(experts, dtype=jnp.int32)[None, :]).astype(jnp.int32)
    position = jnp.sum(jnp.cumsum(onehot, axis=0) * onehot, axis=1) - 1
    slot_index = (flat_ids * slots + position).reshape(rows, 2)
    targets = jnp.arange(experts * slots, dtype=jnp.int32)
    placing = jnp.any(slot_index[None, :, :] == targets[:, None, None], axis=2).astype(jnp.bfloat16)
    outgoing = jnp.dot(placing, normed, preferred_element_type=jnp.float32).astype(jnp.bfloat16)
    outgoing = outgoing.reshape(experts, slots, model_width)

    def expert_rows(block):
        spread = collect(block, "tp", 0)
        produced = run_expert(
            spread.reshape(-1, model_width),
            expert_gate_matrix,
            expert_up_matrix,
            expert_down_matrix,
        )
        summed = summed_on_arrival(produced.reshape(spread.shape).astype(jnp.bfloat16), "tp", 0)
        return exchange_by_chip(summed.astype(jnp.bfloat16), ("sp_0", "sp_1"), (1, 0), 0, 0)

    expert_out = items_in_groups(outgoing, SP, 0, 0, expert_rows, 1, 1)
    flat_out = expert_out.reshape(experts * slots, model_width)
    picked = jnp.take(flat_out, slot_index, axis=0).astype(jnp.float32)
    routed = jnp.sum(chosen_expert_weight[:, :, None] * picked, axis=1)
    return (residual + routed).astype(jnp.bfloat16)


def solution(mesh):
    torus = Mesh(
        mesh.devices.reshape(mesh.shape["grp"], 16, 2, mesh.shape["tp"]),
        ("grp", "sp_0", "sp_1", "tp"),
    )
    return jax.shard_map(
        shards,
        mesh=torus,
        in_specs=(
            P(GRP_SP, "tp"),
            P(GRP_SP, "tp"),
            P(GRP_SP, "tp"),
            P("tp", GRP_SP),
            P("tp", GRP_SP),
            P("tp", GRP_SP),
            P("tp"),
            P("tp", SP),
            P(GRP_SP_TP, None),
            P(),
            P(GRP_SP_TP, None),
            P(GRP_SP_TP, None),
            P(SP, None, "tp"),
            P(SP, None, "tp"),
            P(SP, "tp", None),
        ),
        out_specs=P(GRP_SP_TP, None),
        check_vma=False,
    )
```

profile of v0, /device:TPU:40, one launch (start us, length us, event | category | flops | bytes accessed | tf_op | source)
XLA Modules:
  0.0 451.1 jit_solution(10542415822173141416)
XLA Ops:
  6.6 0.8 fusion.49
  7.3 1.2 reduce-window.6
  8.6 0.1 copy.82
  8.8 0.1 copy.83
  9.0 0.2 slice_reduce_fusion
  9.2 0.9 fusion.55
  10.0 0.8 exponential_bitcast_fusion
  10.8 1.0 copy.81
  11.8 0.5 fusion.27
  12.3 0.7 maximum_bitcast_fusion
  13.1 0.7 all-gather.5.cloned.1.call-update
  13.9 0.7 bitcast_convert_fusion
  14.6 1.0 copy.80
  15.6 0.8 copy.88
  16.3 0.1 eq.28
  16.5 1.1 fusion.25
  17.6 80.7 %all-gather.7.cloned.1.call-done = f32[32,258,128]{2,1,0:T(8,128)} async-done(((f32[1,258,128]{2,1,0:T(8,128)}), f32[32,258,128]{2,1,0:T(8,128)}) %all-gather.7.cloned.1.call-update) | async-done | bytes 4227088 | tf_op jit(solution)/shard_map/all_gather | solution.py:24
  98.2 4.6 %slice.46 = f32[32,256,128]{2,1,0:T(8,128)} slice(f32[32,258,128]{2,1,0:T(8,128)} %all-gather.7.cloned.1.call-done), slice={[0:32], [0:256], [0:128]} | slice | bytes 8388608 | tf_op jit(solution)/shard_map/slice | solution.py:26
  102.9 1.0 fusion.54
  103.9 0.1 multiply_bitcast_fusion
  104.0 0.4 fusion.21
  104.4 0.7 multiply_reduce_fusion.2
  105.2 62.1 %all-gather.5.cloned.1.call-done = bf16[512,2048]{0,1:T(8,128)(2,1)} async-done(((bf16[512,64]{0,1:T(8,128)(2,1)}), bf16[512,2048]{0,1:T(8,128)(2,1)}) %all-gather.5.cloned.1.call-update) | async-done | bytes 2097168 | tf_op jit(solution)/shard_map/all_gather | solution.py:204
  167.4 3.3 convolution_convert_fusion
  170.7 4.3 all-to-all-start
  175.0 0.1 fusion.47
  175.1 0.2 reduce_window_sum.29
  175.2 0.2 select_reduce_fusion
  175.4 0.1 sub.68
  175.6 0.1 fusion.46
  175.7 13.3 %all-to-all-done = bf16[4,56,2048]{2,1,0:T(8,128)(2,1)S(1)} async-done(((bf16[4,56,2048]{2,1,0:T(8,128)(2,1)}), bf16[4,56,2048]{2,1,0:T(8,128)(2,1)S(1)}, u32[]{:S(2)}, u32[]{:S(2)}) %all-to-all-start) | async-done | bytes 917536 | tf_op jit(solution)/shard_map/all_to_all | solution.py:53
  189.0 0.1 convert_reduce_fusion
  189.2 0.2 multiply_reduce_fusion.1
  189.4 0.5 convolution_convert_fusion.1
  189.9 0.3 reshape.114
  190.2 64.3 %all_to_all.30 = bf16[32,7,2048]{2,1,0:T(8,128)(2,1)S(1)} all-to-all(bf16[32,7,2048]{2,1,0:T(8,128)(2,1)S(1)} %reshape.114), channel_id=1, replica_groups=mesh['grp'=2,'sp_0'=16,'sp_1'=2,'tp'=4] {'sp_0','sp_1'}, dimensions={0} | all-to-all | bytes 1835008 | tf_op jit(solution)/shard_map/all_to_all | solution.py:100
  254.5 0.6 copy.91
  255.1 0.5 broadcast_in_dim.53
  255.5 46.2 %all_to_all.31 = bf16[4,32,7,2048]{3,1,2,0:T(8,128)(2,1)S(1)} all-to-all(bf16[4,32,7,2048]{3,1,2,0:T(8,128)(2,1)S(1)} %broadcast_in_dim.53), channel_id=1, replica_groups=mesh['grp'=2,'sp_0'=16,'sp_1'=2,'tp'=4] {'tp'}, dimensions={0} | all-to-all | bytes 7340032 | tf_op jit(solution)/shard_map/all_to_all | solution.py:59
  301.7 4.0 copy.92
  305.7 6.0 %reshape_reshape.10 = bf16[896,2048]{1,0:T(8,128)(2,1)} reshape(bf16[4,32,7,2048]{3,2,1,0:T(8,128)(2,1)} %copy.92) | data formatting | bytes 7340032 | tf_op jit(solution)/shard_map/reshape;reshape | solution.py:227
  311.8 7.2 %fusion.7 = f32[896,896]{1,0:T(8,128)S(1)} fusion(bf16[896,2048]{1,0:T(8,128)(2,1)} %reshape_reshape.10, bf16[1,2048,896]{2,1,0:T(8,128)(2,1)} %param.30), kind=kOutput, calls=%fused_computation.13 | convolution fusion | flops 3288334336 | bytes 10551296 | tf_op jit(solution)/shard_map/dot_general | solution.py:164
  319.0 5.4 %multiply_convert_fusion = bf16[896,896]{1,0:T(8,128)(2,1)} fusion(f32[896,896]{1,0:T(8,128)S(1)} %fusion.7, bf16[896,2048]{1,0:T(8,128)(2,1)S(1)} %copy-done.2, bf16[1,2048,896]{2,1,0:T(8,128)(2,1)S(1)} %copy-done.8), kind=kOutput, calls=%fused_computation.18 | convolution fusion | flops 3293151232 | bytes 12156928 | tf_op jit(solution)/shard_map/dot_general | solution.py:163
  324.4 2.5 dot_general.40
  326.9 6.2 %fusion.11 = bf16[128,7,2048]{2,0,1:T(8,128)(2,1)S(1)} fusion(bf16[1,896,2048]{2,1,0:T(8,128)(2,1)} %param.31, bf16[128,7,896]{2,1,0:T(8,128)(2,1)S(1)} %dot_general.40), kind=kOutput, calls=%fused_computation.17 | convolution fusion | flops 3290169344 | bytes 8945664 | tf_op jit(solution)/shard_map/dot_general | solution.py:166
  333.1 0.5 copy.94
  333.6 46.2 %all_to_all.32 = bf16[4,32,7,2048]{3,1,2,0:T(8,128)(2,1)} all-to-all(bf16[4,32,7,2048]{3,1,2,0:T(8,128)(2,1)S(1)} %copy.94), channel_id=1, replica_groups=mesh['grp'=2,'sp_0'=16,'sp_1'=2,'tp'=4] {'tp'}, dimensions={0} | all-to-all | bytes 7340032 | tf_op jit(solution)/shard_map/all_to_all | solution.py:53
  379.8 2.8 reduce_sum.61
  382.6 0.6 reshape_reshape.11
  383.2 0.3 copy.96
  383.5 4.5 all_to_all.33
  388.0 1.9 copy.97
  389.8 4.3 all-to-all-start.5
  394.1 0.1 copy.99
  394.2 0.1 reshape.119
  394.4 0.1 copy.90
  394.5 0.1 copy.87
  394.6 44.8 %all-to-all-done.5 = bf16[16,2,1,7,2048]{4,1,3,2,0:T(2,128)(2,1)S(1)} async-done(((bf16[16,2,1,7,2048]{4,1,3,2,0:T(2,128)(2,1)}), bf16[16,2,1,7,2048]{4,1,3,2,0:T(2,128)(2,1)S(1)}, u32[]{:S(2)}, u32[]{:S(2)}) %all-to-all-start.5) | async-done | bytes 917536 | tf_op jit(solution)/shard_map/all_to_all | solution.py:77
  439.4 0.4 copy.98
  439.8 0.3 reshape_reshape_reshape.3
  440.1 0.9 gather_fusion
  441.0 0.3 reshape.118
  441.3 2.2 multiply_reduce_fusion
  443.5 0.7 add_convert_fusion
  (41 shorter events, 0.6 us)
Async XLA Ops:
  6.5 5.3 %copy-start = (bf16[224,512]{1,0:T(8,128)(2,1)S(1)}, bf16[224,512]{1,0:T(8,128)(2,1)}, u32[]{:S(2)}) copy-start(bf16[224,512]{1,0:T(8,128)(2,1)} %param.19) | copy-start | bytes 688132
  6.6 91.7 %all-gather.7.cloned.1.call-start = ((), (), s32[]{:S(2)}) async-start(), calls=%async_computation.7 | async-start | bytes 4460544 | tf_op jit(solution)/shard_map/all_gather | solution.py:24
  13.0 154.3 %all-gather.5.cloned.1.call-start = ((), (), s32[]{:S(2)}) async-start(), calls=%async_computation.6 | async-start | bytes 2162688 | tf_op jit(solution)/shard_map/all_gather | solution.py:204
  17.6 86.8 %copy-start.4 = (f32[4,224]{1,0:T(4,128)S(1)}, f32[4,224]{1,0:T(4,128)}, u32[]{:S(2)}) copy-start(f32[4,224]{1,0:T(4,128)} %param.20) | copy-start | bytes 10756
  104.4 71.2 %copy-start.5 = (bf16[2048]{0:T(1024)(128)(2,1)S(1)}, bf16[2048]{0:T(1024)(128)(2,1)}, u32[]{:S(2)}) copy-start(bf16[2048]{0:T(1024)(128)(2,1)} %param.26) | copy-start | bytes 12292
  104.4 71.2 %copy-start.6 = (s32[56,2]{0,1:T(2,128)S(1)}, s32[56,2]{0,1:T(2,128)}, u32[]{:S(2)}) copy-start(s32[56,2]{0,1:T(2,128)} %param.27) | copy-start | bytes 1348
  105.2 84.0 %copy-start.3 = (bf16[56,2048]{1,0:T(8,128)(2,1)S(1)}, bf16[56,2048]{1,0:T(8,128)(2,1)}, u32[]{:S(2)}) copy-start(bf16[56,2048]{1,0:T(8,128)(2,1)} %param.25) | copy-start | bytes 688132
  170.7 18.3 %all-to-all-start = ((bf16[4,56,2048]{2,1,0:T(8,128)(2,1)}), bf16[4,56,2048]{2,1,0:T(8,128)(2,1)S(1)}, u32[]{:S(2)}, u32[]{:S(2)}) async-start(bf16[4,56,2048]{2,1,0:T(8,128)(2,1)} %bitcast.19), calls=%async_computation | async-start | bytes 1835008 | tf_op jit(solution)/shard_map/all_to_all | solution.py:53
  311.8 7.2 %copy-start.2 = (bf16[896,2048]{1,0:T(8,128)(2,1)S(1)}, bf16[896,2048]{1,0:T(8,128)(2,1)}, u32[]{:S(2)}) copy-start(bf16[896,2048]{1,0:T(8,128)(2,1)} %reshape_reshape.10) | copy-start | bytes 11010052
  311.8 7.3 %copy-start.8 = (bf16[1,2048,896]{2,1,0:T(8,128)(2,1)S(1)}, bf16[1,2048,896]{2,1,0:T(8,128)(2,1)}, u32[]{:S(2)}) copy-start(bf16[1,2048,896]{2,1,0:T(8,128)(2,1)} %param.29) | copy-start | bytes 11010052
  383.2 11.3 %copy-start.7 = (f32[56,2]{0,1:T(2,128)S(1)}, f32[56,2]{0,1:T(2,128)}, u32[]{:S(2)}) copy-start(f32[56,2]{0,1:T(2,128)} %param.28) | copy-start | bytes 1348
  389.8 49.6 %all-to-all-start.5 = ((bf16[16,2,1,7,2048]{4,1,3,2,0:T(2,128)(2,1)}), bf16[16,2,1,7,2048]{4,1,3,2,0:T(2,128)(2,1)S(1)}, u32[]{:S(2)}, u32[]{:S(2)}) async-start(bf16[16,2,1,7,2048]{4,1,3,2,0:T(2,128)(2,1)} %copy.97), calls=%async_computation.5 | async-start | bytes 1835008 | tf_op jit(solution)/shard_map/all_to_all | solution.py:77
  439.8 4.5 copy-start.1
Sparse Core Ops, SparseCore 0:
  13.2 85.0 all-gather.6
  100.1 67.2 all-gather.4
where the time goes:
time: 453 us; the launch traced here: 451 us
  waiting for transfers between devices  202 us (45%)
  blocking collectives  161 us (36%)
  local copies, waits for them, and re-layouts  28.6 us (6%)
  matrix products  24.3 us (5%)
  between operations  13.8 us (3%)
  other arithmetic  12.9 us (3%)
  starting transfers between devices  8.63 us (2%)
    all_gather x1, waiting for transfers between devices, all_in_one(): both, at, found = (lax.all_gather(jnp.concatenate(lines), axis), 0, {})  80.7 us
    all_to_all x1, blocking collectives, items_in_groups(): lax.all_to_all(group, axis, split_axis=split_dim, concat_axis=concat_dim,...  64.3 us
    all_gather x1, waiting for transfers between devices, shards(): lax.all_gather(cell_output_matrix, SP, axis=1, tiled=True)  62.1 us
    all_to_all x1, blocking collectives, from_everyone(): return lax.all_to_all(copies, axis, split_axis=0, concat_axis=0, tiled=True)  46.2 us
    all_to_all x1, blocking collectives, summed_on_arrival(): tiles = lax.all_to_all(cut_along(x, dim, size), axis, 0, 0, tiled=True)  46.2 us
    all_to_all x1, waiting for transfers between devices, exchange_in_order(): lax.all_to_all(tiles, axes[k], split_axis=k, concat_axis=k, tiled=True)  44.8 us
    all_to_all x1, waiting for transfers between devices, summed_on_arrival(): tiles = lax.all_to_all(cut_along(x, dim, size), axis, 0, 0, tiled=True)  13.3 us
  transfers between devices with their start and end apart: 4, of which 4 were waited for; matrix products, arithmetic and copies ran while one was open for 3% of the time, Pallas kernels for 0%

commit v1 on v0

--- a/solution.py
+++ b/solution.py
@@ -201,7 +201,12 @@
     )
     partial_value = jnp.dot(
         mixed,
-        lax.all_gather(cell_output_matrix, SP, axis=1, tiled=True),
+        jnp.concatenate(
+            lax.all_to_all(
+                jnp.stack([cell_output_matrix for _ in range(lax.psum(1, SP))], axis=0), SP, 0, 0
+            ),
+            1,
+        ),
         preferred_element_type=jnp.float32,
     )
     projected = summed_on_arrival(partial_value.astype(jnp.bfloat16), "tp", 0)

time: 453 us -> 475 us (1.049)
  blocking collectives: 161 us -> 189 us
  waiting for transfers between devices: 202 us -> 175 us
  starting transfers between devices: 8.63 us -> 33.3 us
    all_gather x1 -> x0, waiting for transfers between devices: 62.1 us -> none  [shards(): lax.all_gather(cell_output_matrix, SP, axis=1, tiled=True)]
    all_gather x1, waiting for transfers between devices: 80.7 us -> 115 us  [all_in_one(): both, at, found = (lax.all_gather(jnp.concatenate(lines), axis), 0, {})]
    all_to_all x1, blocking collectives: 64.3 us -> 91.9 us  [items_in_groups(): lax.all_to_all(group, axis, split_axis=split_dim, concat_axis=concat_dim,...]
    all_to_all x0 -> x1, starting transfers between devices: none -> 24.7 us  [shards(): lax.all_to_all(jnp.stack([cell_output_matrix for _ in range(lax.psum(1, S...]
  transfers between devices with their start and end apart: 4 -> 4, of which waited for: 4 -> 3; matrix products, arithmetic and copies ran while one was open for 3% -> 3% of each run, Pallas kernels for 0% -> 0%
where the time goes in v1:
time: 475 us; the launch traced here: 474 us
  blocking collectives  189 us (40%)
  waiting for transfers between devices  175 us (37%)
  starting transfers between devices  33.3 us (7%)
  local copies, waits for them, and re-layouts  29.1 us (6%)
  matrix products  22.7 us (5%)
  between operations  13.9 us (3%)
  other arithmetic  11.5 us (2%)
    all_gather x1, waiting for transfers between devices, all_in_one(): both, at, found = (lax.all_gather(jnp.concatenate(lines), axis), 0, {})  115 us
    all_to_all x1, blocking collectives, items_in_groups(): lax.all_to_all(group, axis, split_axis=split_dim, concat_axis=concat_dim,...  91.9 us
    all_to_all x1, blocking collectives, from_everyone(): return lax.all_to_all(copies, axis, split_axis=0, concat_axis=0, tiled=True)  46.2 us
    all_to_all x1, blocking collectives, summed_on_arrival(): tiles = lax.all_to_all(cut_along(x, dim, size), axis, 0, 0, tiled=True)  46.2 us
    all_to_all x1, waiting for transfers between devices, exchange_in_order(): lax.all_to_all(tiles, axes[k], split_axis=k, concat_axis=k, tiled=True)  45.3 us
    all_to_all x1, starting transfers between devices, shards(): lax.all_to_all(jnp.stack([cell_output_matrix for _ in range(lax.psum(1, S...  24.7 us
    all_to_all x1, waiting for transfers between devices, summed_on_arrival(): tiles = lax.all_to_all(cut_along(x, dim, size), axis, 0, 0, tiled=True)  14.3 us
  transfers between devices with their start and end apart: 4, of which 3 were waited for; matrix products, arithmetic and copies ran while one was open for 3% of the time, Pallas kernels for 0%

profile of v1, /device:TPU:40, one launch (start us, length us, event | category | flops | bytes accessed | tf_op | source)
XLA Modules:
  0.0 474.0 jit_solution(7300180685984158342)
XLA Ops:
  6.6 0.8 fusion.49
  7.3 1.2 reduce-window.6
  8.6 0.1 copy.83
  8.8 0.1 copy.84
  9.0 0.2 slice_reduce_fusion
  9.2 0.9 fusion.55
  10.0 0.8 exponential_bitcast_fusion
  10.8 1.0 copy.82
  11.9 0.5 fusion.27
  12.4 0.7 maximum_bitcast_fusion
  13.1 2.4 stack.2
  15.5 24.7 %all-to-all-start = ((bf16[32,512,64]{1,2,0:T(8,128)(2,1)}), bf16[32,512,64]{1,2,0:T(8,128)(2,1)S(1)}, u32[]{:S(2)}, u32[]{:S(2)}) async-start(bf16[32,512,64]{1,2,0:T(8,128)(2,1)} %stack.2), calls=%async_computation | async-start | bytes 4194304 | tf_op jit(solution)/shard_map/all_to_all | solution.py:205
  40.3 0.1 copy.81
  40.4 0.1 copy.89
  40.5 0.1 eq.28
  40.7 0.6 copy-done.5
  41.3 0.4 fusion.25
  41.7 115.1 %all-gather.4.cloned.1.call-done = f32[32,258,128]{2,1,0:T(8,128)} async-done(((f32[1,258,128]{2,1,0:T(8,128)}), f32[32,258,128]{2,1,0:T(8,128)}) %all-gather.4.cloned.1.call-update) | async-done | bytes 4227088 | tf_op jit(solution)/shard_map/all_gather | solution.py:24
  156.8 4.6 slice.46
  161.4 1.0 fusion.54
  162.5 0.1 multiply_bitcast_fusion
  162.5 0.4 fusion.21
  163.0 1.7 multiply_reduce_fusion.2
  164.6 1.8 convolution_convert_fusion
  166.4 4.4 all-to-all-start.1
  170.8 0.1 fusion.47
  170.9 0.2 reduce_window_sum.29
  171.1 0.2 select_reduce_fusion
  171.3 0.1 sub.68
  171.5 0.1 fusion.46
  171.6 14.3 %all-to-all-done.1 = bf16[4,56,2048]{2,1,0:T(8,128)(2,1)S(1)} async-done(((bf16[4,56,2048]{2,1,0:T(8,128)(2,1)}), bf16[4,56,2048]{2,1,0:T(8,128)(2,1)S(1)}, u32[]{:S(2)}, u32[]{:S(2)}) %all-to-all-start.1) | async-done | bytes 917536 | tf_op jit(solution)/shard_map/all_to_all | solution.py:53
  185.9 0.1 convert_reduce_fusion
  186.0 0.2 multiply_reduce_fusion.1
  186.2 0.5 convolution_convert_fusion.1
  186.7 0.3 reshape.124
  187.0 91.9 %all_to_all.35 = bf16[32,7,2048]{2,1,0:T(8,128)(2,1)S(1)} all-to-all(bf16[32,7,2048]{2,1,0:T(8,128)(2,1)S(1)} %reshape.124), channel_id=1, replica_groups=mesh['grp'=2,'sp_0'=16,'sp_1'=2,'tp'=4] {'sp_0','sp_1'}, dimensions={0} | all-to-all | bytes 1835008 | tf_op jit(solution)/shard_map/all_to_all | solution.py:100
  278.9 0.6 copy.92
  279.5 0.5 broadcast_in_dim.53
  279.9 46.2 %all_to_all.36 = bf16[4,32,7,2048]{3,1,2,0:T(8,128)(2,1)S(1)} all-to-all(bf16[4,32,7,2048]{3,1,2,0:T(8,128)(2,1)S(1)} %broadcast_in_dim.53), channel_id=1, replica_groups=mesh['grp'=2,'sp_0'=16,'sp_1'=2,'tp'=4] {'tp'}, dimensions={0} | all-to-all | bytes 7340032 | tf_op jit(solution)/shard_map/all_to_all | solution.py:59
  326.1 4.0 copy.93
  330.1 6.0 %reshape_reshape.10 = bf16[896,2048]{1,0:T(8,128)(2,1)} reshape(bf16[4,32,7,2048]{3,2,1,0:T(8,128)(2,1)} %copy.93) | data formatting | bytes 7340032 | tf_op jit(solution)/shard_map/reshape;reshape | solution.py:232
  336.1 7.2 %fusion.7 = f32[896,896]{1,0:T(8,128)S(1)} fusion(bf16[896,2048]{1,0:T(8,128)(2,1)} %reshape_reshape.10, bf16[1,2048,896]{2,1,0:T(8,128)(2,1)} %param.30), kind=kOutput, calls=%fused_computation.13 | convolution fusion | flops 3288334336 | bytes 10551296 | tf_op jit(solution)/shard_map/dot_general | solution.py:164
  343.4 4.2 multiply_convert_fusion
  347.6 1.5 dot_general.40
  349.1 6.5 %fusion.11 = bf16[128,7,2048]{2,0,1:T(8,128)(2,1)S(1)} fusion(bf16[1,896,2048]{2,1,0:T(8,128)(2,1)} %param.31, bf16[128,7,896]{2,1,0:T(8,128)(2,1)} %dot_general.40), kind=kOutput, calls=%fused_computation.17 | convolution fusion | flops 3290169344 | bytes 8945664 | tf_op jit(solution)/shard_map/dot_general | solution.py:166
  355.7 0.5 copy.95
  356.2 46.2 %all_to_all.37 = bf16[4,32,7,2048]{3,1,2,0:T(8,128)(2,1)} all-to-all(bf16[4,32,7,2048]{3,1,2,0:T(8,128)(2,1)S(1)} %copy.95), channel_id=1, replica_groups=mesh['grp'=2,'sp_0'=16,'sp_1'=2,'tp'=4] {'tp'}, dimensions={0} | all-to-all | bytes 7340032 | tf_op jit(solution)/shard_map/all_to_all | solution.py:53
  402.3 2.8 reduce_sum.61
  405.1 0.6 reshape_reshape.11
  405.7 0.3 copy.97
  406.0 4.5 all_to_all.38
  410.5 1.9 copy.98
  412.4 4.1 all-to-all-start.6
  416.5 0.1 copy.100
  416.6 0.1 reshape.129
  416.7 0.1 copy.91
  416.8 0.1 copy.88
  416.9 45.3 %all-to-all-done.6 = bf16[16,2,1,7,2048]{4,1,3,2,0:T(2,128)(2,1)S(1)} async-done(((bf16[16,2,1,7,2048]{4,1,3,2,0:T(2,128)(2,1)}), bf16[16,2,1,7,2048]{4,1,3,2,0:T(2,128)(2,1)S(1)}, u32[]{:S(2)}, u32[]{:S(2)}) %all-to-all-start.6) | async-done | bytes 917536 | tf_op jit(solution)/shard_map/all_to_all | solution.py:77
  462.3 0.4 copy.99
  462.6 0.3 reshape_reshape_reshape.3
  463.0 0.9 gather_fusion
  463.9 0.3 reshape.128
  464.2 2.2 multiply_reduce_fusion
  466.4 0.7 add_convert_fusion
  (51 shorter events, 0.5 us)
Async XLA Ops:
  6.5 5.3 %copy-start = (bf16[224,512]{1,0:T(8,128)(2,1)S(1)}, bf16[224,512]{1,0:T(8,128)(2,1)}, u32[]{:S(2)}) copy-start(bf16[224,512]{1,0:T(8,128)(2,1)} %param.19) | copy-start | bytes 688132
  6.6 150.2 %all-gather.4.cloned.1.call-start = ((), (), s32[]{:S(2)}) async-start(), calls=%async_computation.7 | async-start | bytes 4460544 | tf_op jit(solution)/shard_map/all_gather | solution.py:24
  11.8 3.7 copy-start.6
  11.8 28.5 %copy-start.7 = (bf16[224,256]{1,0:T(8,128)(2,1)S(1)}, bf16[224,256]{1,0:T(8,128)(2,1)}, u32[]{:S(2)}) copy-start(bf16[224,256]{1,0:T(8,128)(2,1)} %param.17) | copy-start | bytes 344068
  11.8 28.6 %copy-start.10 = (s32[56,2]{0,1:T(2,128)S(1)}, s32[56,2]{0,1:T(2,128)}, u32[]{:S(2)}) copy-start(s32[56,2]{0,1:T(2,128)} %param.27) | copy-start | bytes 1348
  12.3 29.0 %copy-start.8 = (f32[4,224]{1,0:T(4,128)S(1)}, f32[4,224]{1,0:T(4,128)}, u32[]{:S(2)}) copy-start(f32[4,224]{1,0:T(4,128)} %param.20) | copy-start | bytes 10756
  12.4 29.3 %copy-start.11 = (bf16[512]{0:T(512)(128)(2,1)S(1)}, bf16[512]{0:T(512)(128)(2,1)}, u32[]{:S(2)}) copy-start(bf16[512]{0:T(512)(128)(2,1)} %param.23) | copy-start | bytes 3076
  15.5 149.1 %all-to-all-start = ((bf16[32,512,64]{1,2,0:T(8,128)(2,1)}), bf16[32,512,64]{1,2,0:T(8,128)(2,1)S(1)}, u32[]{:S(2)}, u32[]{:S(2)}) async-start(bf16[32,512,64]{1,2,0:T(8,128)(2,1)} %stack.2), calls=%async_computation | async-start | bytes 4194304 | tf_op jit(solution)/shard_map/all_to_all | solution.py:205
  40.7 0.6 copy-start.5
  162.9 8.5 %copy-start.9 = (bf16[2048]{0:T(1024)(128)(2,1)S(1)}, bf16[2048]{0:T(1024)(128)(2,1)}, u32[]{:S(2)}) copy-start(bf16[2048]{0:T(1024)(128)(2,1)} %param.26) | copy-start | bytes 12292
  164.6 21.4 %copy-start.3 = (bf16[56,2048]{1,0:T(8,128)(2,1)S(1)}, bf16[56,2048]{1,0:T(8,128)(2,1)}, u32[]{:S(2)}) copy-start(bf16[56,2048]{1,0:T(8,128)(2,1)} %param.25) | copy-start | bytes 688132
  166.4 19.5 %all-to-all-start.1 = ((bf16[4,56,2048]{2,1,0:T(8,128)(2,1)}), bf16[4,56,2048]{2,1,0:T(8,128)(2,1)S(1)}, u32[]{:S(2)}, u32[]{:S(2)}) async-start(bf16[4,56,2048]{2,1,0:T(8,128)(2,1)} %bitcast.21), calls=%async_computation.1 | async-start | bytes 1835008 | tf_op jit(solution)/shard_map/all_to_all | solution.py:53
  336.1 7.2 %copy-start.2 = (bf16[896,2048]{1,0:T(8,128)(2,1)S(1)}, bf16[896,2048]{1,0:T(8,128)(2,1)}, u32[]{:S(2)}) copy-start(bf16[896,2048]{1,0:T(8,128)(2,1)} %reshape_reshape.10) | copy-start | bytes 11010052
  336.1 7.2 %copy-start.13 = (bf16[1,2048,896]{2,1,0:T(8,128)(2,1)S(1)}, bf16[1,2048,896]{2,1,0:T(8,128)(2,1)}, u32[]{:S(2)}) copy-start(bf16[1,2048,896]{2,1,0:T(8,128)(2,1)} %param.29) | copy-start | bytes 11010052
  405.7 11.1 %copy-start.12 = (f32[56,2]{0,1:T(2,128)S(1)}, f32[56,2]{0,1:T(2,128)}, u32[]{:S(2)}) copy-start(f32[56,2]{0,1:T(2,128)} %param.28) | copy-start | bytes 1348
  412.4 49.9 %all-to-all-start.6 = ((bf16[16,2,1,7,2048]{4,1,3,2,0:T(2,128)(2,1)}), bf16[16,2,1,7,2048]{4,1,3,2,0:T(2,128)(2,1)S(1)}, u32[]{:S(2)}, u32[]{:S(2)}) async-start(bf16[16,2,1,7,2048]{4,1,3,2,0:T(2,128)(2,1)} %copy.98), calls=%async_computation.6 | async-start | bytes 1835008 | tf_op jit(solution)/shard_map/all_to_all | solution.py:77
  462.6 3.8 copy-start.4
  462.6 4.5 copy-start.1
Sparse Core Ops, SparseCore 0:
  13.2 143.5 all-gather.3
